TPU v7x, 32 devices: a whole 2x2x4 slice. The times are simulated.
32 devices in a mesh: sp: 16 (over z, y, core), tp: 2 (over x).
Axes of the slice: x: 2, y: 2, z: 4, core: 2. Of those that a mesh axis runs over, the one named last changes fastest.
Arguments:
- tokens: bfloat16 [2048, 2048], P(('sp', 'tp')), may hold values from -16 to 16
- w_query: bfloat16 [2048, 1024], P(None, 'tp'), may hold values from -0.110485435 to 0.110485435
- w_key: bfloat16 [2048, 256], P(None, 'tp'), may hold values from -0.15467961 to 0.15467961
- w_value: bfloat16 [2048, 256], P(None, 'tp'), may hold values from -0.125 to 0.125
- cum_gate: float32 [2048, 16], P('sp', 'tp'), may hold values from -371 to 0, as said below
- w_out: bfloat16 [1024, 2048], replicated, may hold values from -0.1875 to 0.1875
Outputs:
- mixed: bfloat16 [2048, 2048], P(('sp', 'tp'))
Inputs may be any that keep to these rules, and one draw needn't show every extreme that they name: `cum_gate`: each head's column does not rise along the positions.
All inputs are finite; a program needn't handle non-finite values.
Results may differ from a plain program's by a relative error of at most 0.012.
Values may be sent and summed in bfloat16 or wider, within the bound.
A program may use at most 64 MiB of HBM per device.

v0:
```python
import math
import jax
import jax.numpy as jnp
from jax import lax
from jax.sharding import PartitionSpec as P

HEAD_DIM = 64
NEG_FILL = -1e30


def shards(tokens, w_query, w_key, w_value, cum_gate, w_out):
    query_cols = w_query.shape[1]
    pair_cols = w_key.shape[1]
    local_heads = query_cols // HEAD_DIM
    local_kv = pair_cols // HEAD_DIM
    group = local_heads // local_kv
    stacked = jnp.concatenate((w_query, w_key, w_value), axis=1)
    joined = jnp.dot(
        lax.all_gather(tokens, "tp", axis=0, tiled=True),
        stacked,
        preferred_element_type=jnp.float32,
    ).astype(jnp.bfloat16)
    row_count = joined.shape[0]
    queries = joined[:, :query_cols].reshape(row_count, local_kv, group, HEAD_DIM)
    keys = joined[:, query_cols : query_cols + pair_cols]
    values = joined[:, query_cols + pair_cols :]
    gate_query = cum_gate.reshape(row_count, local_kv, group)
    gate_every = lax.all_gather(cum_gate, "sp", axis=0, tiled=True)
    keys_every, values_every = (
        lax.all_gather(keys, "sp", axis=0, tiled=True),
        lax.all_gather(values, "sp", axis=0, tiled=True),
    )
    length = keys_every.shape[0]
    width = math.gcd(length, 2048)
    position_shift = lax.axis_index("sp") * row_count
    query_pos = position_shift + jnp.arange(row_count, dtype=jnp.int32)
    last_pos = position_shift + row_count - 1
    scale = HEAD_DIM ** (-0.5)

    def add_block(index, state):
        run_max, run_total, run_acc = state
        block_start = index * width
        key_block = lax.dynamic_slice_in_dim(keys_every, block_start, width, 0)
        value_block = lax.dynamic_slice_in_dim(values_every, block_start, width, 0)
        gate_block = lax.dynamic_slice_in_dim(gate_every, block_start, width, 0)
        gate_key = gate_block.reshape(width, local_kv, group).transpose(1, 2, 0)
        scores = jnp.einsum(
            "tkgd,rkd->tkgr",
            queries,
            key_block.reshape(width, local_kv, HEAD_DIM),
            preferred_element_type=jnp.float32,
        )
        scores = scores * scale + gate_query[..., None] - gate_key[None]
        key_pos = block_start + jnp.arange(width, dtype=jnp.int32)
        allowed = (key_pos[None, :] <= query_pos[:, None])[:, None, None, :]
        scores = jnp.where(allowed, scores, NEG_FILL)
        new_max = jnp.maximum(run_max, jnp.max(scores, axis=-1))
        weights = jnp.where(allowed, jnp.exp(scores - new_max[..., None]), 0.0)
        factor = jnp.exp(run_max - new_max)
        new_total = run_total * factor + jnp.sum(weights, axis=-1)
        gained = jnp.einsum(
            "tkgr,rkd->tkgd",
            weights.astype(jnp.bfloat16),
            value_block.reshape(width, local_kv, HEAD_DIM),
            preferred_element_type=jnp.float32,
        )
        return (new_max, new_total, run_acc * factor[..., None] + gained)

    initial = (
        jnp.full((row_count, local_kv, group), NEG_FILL, jnp.float32),
        jnp.zeros((row_count, local_kv, group), jnp.float32),
        jnp.zeros((row_count, local_kv, group, HEAD_DIM), jnp.float32),
    )
    run_max, run_total, run_acc = lax.fori_loop(0, last_pos // width + 1, add_block, initial)
    attended = (run_acc / run_total[..., None]).astype(jnp.bfloat16).reshape(row_count, query_cols)
    regrouped = lax.all_to_all(attended, "tp", split_axis=0, concat_axis=1, tiled=True)
    return jnp.dot(regrouped, w_out, preferred_element_type=jnp.float32).astype(jnp.bfloat16)


def solution(mesh):
    placed = (
        P(("sp", "tp"), None),
        P(None, "tp"),
        P(None, "tp"),
        P(None, "tp"),
        P("sp", "tp"),
        P(),
    )
    return jax.shard_map(
        shards, mesh=mesh, in_specs=placed, out_specs=P(("sp", "tp"), None), check_vma=False
    )
```

profile of v0, /device:TPU:0, one launch (start us, length us, event | category | flops | bytes accessed | tf_op | source)
XLA Modules:
  0.0 94.7 jit_solution(8654843042355154446)
XLA Ops:
  0.0 0.0 copy-start.1
  0.0 10.3 %all_gather.12 = bf16[128,2048]{1,0:T(8,128)(2,1)S(1)} all-gather(bf16[64,2048]{1,0:T(8,128)(2,1)} %param.8), channel_id=1, replica_groups=mesh['sp'=16,'tp'=2] {'tp'}, dimensions={0}, use_global_device_ids=true | all-gather | bytes 786432 | tf_op jit(solution)/shard_map/all_gather | solution.py:19
  10.3 3.0 %fusion.28 = bf16[128,768]{0,1:T(8,128)(2,1)S(1)} fusion(bf16[128,2048]{1,0:T(8,128)(2,1)S(1)} %all_gather.12, bf16[2048,128]{1,0:T(8,128)(2,1)} %param.11, bf16[2048,128]{1,0:T(8,128)(2,1)} %param.10, bf16[2048,512]{1,0:T(8,128)(2,1)} %param.9), kind=kOutput, calls=%fused_computation.28 | convolution fusion | flops 412188672 | bytes 3866624 | tf_op jit(solution)/shard_map/dot_general | solution.py:18
  13.3 0.0 copy-done.1
  13.3 22.0 %all_gather.14 = f32[2048,8]{0,1:T(8,128)S(1)} all-gather(f32[128,8]{0,1:T(8,128)S(1)} %copy-done.1), channel_id=1, replica_groups=mesh['sp'=16,'tp'=2] {'sp'}, dimensions={0}, use_global_device_ids=true | all-gather | bytes 69632 | tf_op jit(solution)/shard_map/all_gather | solution.py:28
  35.3 0.0 copy-start
  35.4 18.9 %all_gather.15 = bf16[2048,128]{0,1:T(8,128)(2,1)S(1)} all-gather(bf16[128,128]{0,1:T(8,128)(2,1)S(1)} %get-tuple-element.118), channel_id=1, replica_groups=mesh['sp'=16,'tp'=2] {'sp'}, dimensions={0}, use_global_device_ids=true | all-gather | bytes 557056 | tf_op jit(solution)/shard_map/all_gather | solution.py:31
  54.3 20.3 %all_gather.13 = bf16[2048,128]{0,1:T(8,128)(2,1)S(1)} all-gather(bf16[128,128]{0,1:T(8,128)(2,1)S(1)} %get-tuple-element.119), channel_id=1, replica_groups=mesh['sp'=16,'tp'=2] {'sp'}, dimensions={0}, use_global_device_ids=true | all-gather | bytes 557056 | tf_op jit(solution)/shard_map/all_gather | solution.py:30
  74.6 0.0 copy-done
  74.6 9.0 %while.16 = (s32[]{:T(128)}, f32[128,2,4]{0,2,1:T(4,128)S(1)}, f32[128,2,4]{0,2,1:T(4,128)S(1)}, f32[128,2,4,64]{0,3,2,1:T(8,128)S(1)}, s32[]{:T(128)}, /*index=...) while((s32[]{:T(128)}, f32[128,2,4]{0,2,1:T(4,128)S(1)}, ...), condition=%wide.wide.region_3.4_spmd.clone, body=%wide.wide.region_0.3_spmd.clone.sunk | while | flops 577114240 | bytes 28210328 | solution.py:74
  74.6 0.3 broadcast_compare_fusion.3
  75.0 2.6 %fusion.57 = (f32[128,2,4]{0,2,1:T(4,128)S(1)}, f32[2,2048,128,4]{2,1,3,0:T(8,128)S(1)}) fusion(f32[2,4,2048]{2,1,0:T(4,128)S(1)} %bitcast.108, f32[128,2,4]{0,2,1:T(4,128)S(1)} %bitcast.120, pred[128,2048]{0,1:T(8,128)(4,1)S(1)} %broadcast_compare_fusion.3, bf16[2048,2,64,1]{0,2,3,1:T(8,128)(2,1)S(1)} %bitcast.114, ...), kind=kOutput, calls=%fused_computation.7.clone.clone.1 | convolution fusion | flops 278920192 | bytes 9379840 | tf_op jit(solution)/shard_map/while/body/tkgd,rkd->tkgr/dot_general | solution.py:47
  77.6 3.1 %fusion.58 = f32[128,2,4]{0,2,1:T(4,128)S(1)} fusion(f32[2,2048,128,4]{2,1,3,0:T(8,128)S(1)} %get-tuple-element.252, f32[128,2,4]{0,2,1:T(4,128)S(1)} %max.6, f32[2,4,2048]{2,1,0:T(4,128)S(1)} %bitcast.109, f32[128,2,4]{0,2,1:T(4,128)S(1)} %bitcast.121, pred[128,2048]{0,1:T(8,128)(4,1)S(1)} %broadcast_compare_fusion.3), kind=kLoop, calls=%fused_computation.6.clone.clone.1 | loop fusion | flops 14679040 | bytes 8728576 | tf_op jit(solution)/shard_map/while/body/reduce_sum | solution.py:60
  80.8 2.8 %fusion.59 = f32[128,2,4,64]{0,3,2,1:T(8,128)S(1)} fusion(bf16[2048,2,64,1]{0,2,3,1:T(8,128)(2,1)S(1)} %bitcast.113, f32[2,2048,128,4]{2,1,3,0:T(8,128)S(1)} %get-tuple-element.252, f32[128,2,4]{0,2,1:T(4,128)S(1)} %max.6, f32[2,4,2048]{2,1,0:T(4,128)S(1)} %bitcast.110, f32[128,2,4]{0,2,1:T(4,128)S(1)} %bitcast.122, ...), kind=kOutput, calls=%fused_computation.11.clone.clone.1 | convolution fusion | flops 283246592 | bytes 9777152 | tf_op jit(solution)/shard_map/while/body/tkgr,rkd->tkgd/dot_general | solution.py:61
  83.6 0.1 reshape.55
  83.8 0.1 copy.14
  83.9 7.0 %all_to_all.19 = bf16[2,64,512]{2,1,0:T(8,128)(2,1)S(1)} all-to-all(bf16[2,64,512]{2,1,0:T(8,128)(2,1)S(1)} %copy.14), channel_id=1, replica_groups=mesh['sp'=16,'tp'=2] {'tp'}, dimensions={0} | all-to-all | bytes 262144 | tf_op jit(solution)/shard_map/all_to_all | solution.py:76
  91.0 3.7 %convolution_convert_fusion = bf16[64,2048]{1,0:T(8,128)(2,1)} fusion(bf16[64,1024]{1,0:T(8,128)(2,1)S(1)} %bitcast.112, bf16[1024,2048]{1,0:T(8,128)(2,1)} %param.13), kind=kOutput, calls=%fused_computation.26 | convolution fusion | flops 268566528 | bytes 4587520 | tf_op jit(solution)/shard_map/dot_general | solution.py:77
  (13 shorter events, 0.1 us)
Async XLA Ops:
  0.0 13.3 %copy-start.1 = (f32[128,8]{0,1:T(8,128)S(1)}, f32[128,8]{0,1:T(8,128)}, u32[]{:S(2)}) copy-start(f32[128,8]{0,1:T(8,128)} %param.12) | copy-start | bytes 12292
  35.3 39.2 %copy-start = (f32[2048,8]{0,1:T(8,128)}, f32[2048,8]{0,1:T(8,128)S(1)}, u32[]{:S(2)}) copy-start(f32[2048,8]{0,1:T(8,128)S(1)} %all_gather.14) | copy-start | bytes 196612
where the time goes:
time: 94.9 us; the launch traced here: 94.7 us
  blocking collectives  78.5 us (83%)
  matrix products  12.1 us (13%)
  other arithmetic  3.53 us (4%)
    all_gather x1, blocking collectives, shards(): gate_every = lax.all_gather(cum_gate, 'sp', axis=0, tiled=True)  22 us
    all_gather x1, blocking collectives, shards(): lax.all_gather(keys, 'sp', axis=0, tiled=True)  20.3 us
    all_gather x1, blocking collectives, shards(): lax.all_gather(values, 'sp', axis=0, tiled=True)  18.9 us
    all_gather x1, blocking collectives, shards(): lax.all_gather(tokens, 'tp', axis=0, tiled=True)  10.3 us
    all_to_all x1, blocking collectives, shards(): lax.all_to_all(attended, 'tp', split_axis=0, concat_axis=1, tiled=True)  7.03 us
    dot_general x1, matrix products, shards(): jnp.dot(regrouped, w_out, preferred_element_type=jnp.float32)  3.74 us
    reduce_sum x1, other arithmetic, add_block(): new_total = run_total * factor + jnp.sum(weights, axis=-1)  3.13 us
    dot_general x1, matrix products, shards(): jnp.dot(lax.all_gather(tokens, 'tp', axis=0, tiled=True), stacked, prefer...  2.96 us

commit v1 on v0

--- a/solution.py
+++ b/solution.py
@@ -25,7 +25,12 @@
     keys = joined[:, query_cols : query_cols + pair_cols]
     values = joined[:, query_cols + pair_cols :]
     gate_query = cum_gate.reshape(row_count, local_kv, group)
-    gate_every = lax.all_gather(cum_gate, "sp", axis=0, tiled=True)
+    ring = [cum_gate]
+    for hop in range(15):
+        ring.append(lax.ppermute(ring[-1], "sp", [(dev, (dev + 1) % 16) for dev in range(16)]))
+    gate_every = jnp.roll(
+        jnp.concatenate(ring[::-1], axis=0), (lax.axis_index("sp") + 1) * ring[0].shape[0], axis=0
+    )
     keys_every, values_every = (
         lax.all_gather(keys, "sp", axis=0, tiled=True),
         lax.all_gather(values, "sp", axis=0, tiled=True),

time: 94.9 us -> 139 us (1.46)
  waiting for transfers between devices: 0 us -> 66.6 us
  blocking collectives: 78.5 us -> 54.4 us
    ppermute x0 -> x15, waiting for transfers between devices: none -> 66.6 us  [shards(): lax.ppermute(ring[-1], 'sp', [(dev, (dev + 1) % 16) for dev in range(16)])]
    all_gather x1 -> x0, blocking collectives: 22 us -> none  [shards(): gate_every = lax.all_gather(cum_gate, 'sp', axis=0, tiled=True)]
    all_gather x1, blocking collectives: 10.3 us -> 7.24 us  [shards(): lax.all_gather(tokens, 'tp', axis=0, tiled=True)]
  transfers between devices with their start and end apart: 0 -> 15, of which waited for: 0 -> 12; matrix products, arithmetic and copies ran while one was open for 0% -> 2% of each run, Pallas kernels for 0% -> 0%
where the time goes in v1:
time: 139 us
  waiting for transfers between devices  66.6 us (48%)
  blocking collectives  54.4 us (39%)
  matrix products  12.1 us (9%)
  other arithmetic  3.53 us (3%)
    ppermute x15, waiting for transfers between devices, shards(): lax.ppermute(ring[-1], 'sp', [(dev, (dev + 1) % 16) for dev in range(16)])  66.6 us
    all_gather x1, blocking collectives, shards(): lax.all_gather(keys, 'sp', axis=0, tiled=True)  20.4 us
    all_gather x1, blocking collectives, shards(): lax.all_gather(values, 'sp', axis=0, tiled=True)  19.4 us
    all_to_all x1, blocking collectives, shards(): lax.all_to_all(attended, 'tp', split_axis=0, concat_axis=1, tiled=True)  7.4 us
    all_gather x1, blocking collectives, shards(): lax.all_gather(tokens, 'tp', axis=0, tiled=True)  7.24 us
    dot_general x1, matrix products, shards(): jnp.dot(regrouped, w_out, preferred_element_type=jnp.float32)  3.74 us
    reduce_sum x1, other arithmetic, add_block(): new_total = run_total * factor + jnp.sum(weights, axis=-1)  3.13 us
    dot_general x1, matrix products, shards(): jnp.dot(lax.all_gather(tokens, 'tp', axis=0, tiled=True), stacked, prefer...  2.96 us
  transfers between devices with their start and end apart: 15, of which 12 were waited for; matrix products, arithmetic and copies ran while one was open for 2% of the time, Pallas kernels for 0%

profile of v1, /device:TPU:0, one launch (start us, length us, event | category | flops | bytes accessed | tf_op | source)
XLA Modules:
  0.0 138.8 jit_solution(2529899165938277782)
XLA Ops:
  0.0 0.0 copy-start.1
  0.0 0.5 collective-permute-start
  0.5 6.6 %collective-permute-done = f32[128,8]{0,1:T(8,128)S(1)} collective-permute-done((f32[128,8]{0,1:T(8,128)}, f32[128,8]{0,1:T(8,128)S(1)}, u32[]{:S(2)}, u32[]{:S(2)}) %collective-permute-start) | collective-permute-done | bytes 4128 | tf_op jit(solution)/shard_map/ppermute | solution.py:30
  7.0 0.0 collective-permute-start.1
  7.0 5.7 %collective-permute-done.1 = f32[128,8]{0,1:T(8,128)S(1)} collective-permute-done((f32[128,8]{0,1:T(8,128)S(1)}, f32[128,8]{0,1:T(8,128)S(1)}, u32[]{:S(2)}, u32[]{:S(2)}) %collective-permute-start.1) | collective-permute-done | bytes 4128 | tf_op jit(solution)/shard_map/ppermute | solution.py:30
  12.8 0.0 collective-permute-start.2
  12.8 5.7 %collective-permute-done.2 = f32[128,8]{0,1:T(8,128)S(1)} collective-permute-done((f32[128,8]{0,1:T(8,128)S(1)}, f32[128,8]{0,1:T(8,128)S(1)}, u32[]{:S(2)}, u32[]{:S(2)}) %collective-permute-start.2) | collective-permute-done | bytes 4128 | tf_op jit(solution)/shard_map/ppermute | solution.py:30
  18.5 0.0 collective-permute-start.3
  18.5 5.7 %collective-permute-done.3 = f32[128,8]{0,1:T(8,128)S(1)} collective-permute-done((f32[128,8]{0,1:T(8,128)S(1)}, f32[128,8]{0,1:T(8,128)S(1)}, u32[]{:S(2)}, u32[]{:S(2)}) %collective-permute-start.3) | collective-permute-done | bytes 4128 | tf_op jit(solution)/shard_map/ppermute | solution.py:30
  24.2 0.0 collective-permute-start.4
  24.2 5.7 %collective-permute-done.4 = f32[128,8]{0,1:T(8,128)S(1)} collective-permute-done((f32[128,8]{0,1:T(8,128)S(1)}, f32[128,8]{0,1:T(8,128)S(1)}, u32[]{:S(2)}, u32[]{:S(2)}) %collective-permute-start.4) | collective-permute-done | bytes 4128 | tf_op jit(solution)/shard_map/ppermute | solution.py:30
  30.0 0.0 collective-permute-start.5
  30.0 5.7 %collective-permute-done.5 = f32[128,8]{0,1:T(8,128)S(1)} collective-permute-done((f32[128,8]{0,1:T(8,128)S(1)}, f32[128,8]{0,1:T(8,128)S(1)}, u32[]{:S(2)}, u32[]{:S(2)}) %collective-permute-start.5) | collective-permute-done | bytes 4128 | tf_op jit(solution)/shard_map/ppermute | solution.py:30
  35.7 0.0 collective-permute-start.6
  35.7 5.7 %collective-permute-done.6 = f32[128,8]{0,1:T(8,128)S(1)} collective-permute-done((f32[128,8]{0,1:T(8,128)S(1)}, f32[128,8]{0,1:T(8,128)S(1)}, u32[]{:S(2)}, u32[]{:S(2)}) %collective-permute-start.6) | collective-permute-done | bytes 4128 | tf_op jit(solution)/shard_map/ppermute | solution.py:30
  41.4 0.0 collective-permute-start.7
  41.4 5.7 %collective-permute-done.7 = f32[128,8]{0,1:T(8,128)S(1)} collective-permute-done((f32[128,8]{0,1:T(8,128)S(1)}, f32[128,8]{0,1:T(8,128)S(1)}, u32[]{:S(2)}, u32[]{:S(2)}) %collective-permute-start.7) | collective-permute-done | bytes 4128 | tf_op jit(solution)/shard_map/ppermute | solution.py:30
  47.2 0.0 collective-permute-start.8
  47.2 5.7 %collective-permute-done.8 = f32[128,8]{0,1:T(8,128)S(1)} collective-permute-done((f32[128,8]{0,1:T(8,128)S(1)}, f32[128,8]{0,1:T(8,128)S(1)}, u32[]{:S(2)}, u32[]{:S(2)}) %collective-permute-start.8) | collective-permute-done | bytes 4128 | tf_op jit(solution)/shard_map/ppermute | solution.py:30
  52.9 0.0 collective-permute-start.9
  52.9 5.7 %collective-permute-done.9 = f32[128,8]{0,1:T(8,128)S(1)} collective-permute-done((f32[128,8]{0,1:T(8,128)S(1)}, f32[128,8]{0,1:T(8,128)S(1)}, u32[]{:S(2)}, u32[]{:S(2)}) %collective-permute-start.9) | collective-permute-done | bytes 4128 | tf_op jit(solution)/shard_map/ppermute | solution.py:30
  58.6 0.0 collective-permute-start.10
  58.6 7.2 %all_gather.9 = bf16[128,2048]{1,0:T(8,128)(2,1)S(1)} all-gather(bf16[64,2048]{1,0:T(8,128)(2,1)} %param.8), channel_id=1, replica_groups=mesh['sp'=16,'tp'=2] {'tp'}, dimensions={0}, use_global_device_ids=true | all-gather | bytes 786432 | tf_op jit(solution)/shard_map/all_gather | solution.py:19
  65.9 0.0 collective-permute-done.10
  65.9 0.0 collective-permute-start.11
  65.9 3.0 %fusion.28 = bf16[128,768]{0,1:T(8,128)(2,1)S(1)} fusion(bf16[128,2048]{1,0:T(8,128)(2,1)S(1)} %all_gather.9, bf16[2048,128]{1,0:T(8,128)(2,1)} %param.11, bf16[2048,128]{1,0:T(8,128)(2,1)} %param.10, bf16[2048,512]{1,0:T(8,128)(2,1)} %param.9), kind=kOutput, calls=%fused_computation.28 | convolution fusion | flops 412188672 | bytes 3866624 | tf_op jit(solution)/shard_map/dot_general | solution.py:18
  68.8 2.8 %collective-permute-done.11 = f32[128,8]{0,1:T(8,128)S(1)} collective-permute-done((f32[128,8]{0,1:T(8,128)S(1)}, f32[128,8]{0,1:T(8,128)S(1)}, u32[]{:S(2)}, u32[]{:S(2)}) %collective-permute-start.11) | collective-permute-done | bytes 4128 | tf_op jit(solution)/shard_map/ppermute | solution.py:30
  71.6 0.0 collective-permute-start.12
  71.6 5.7 %collective-permute-done.12 = f32[128,8]{0,1:T(8,128)S(1)} collective-permute-done((f32[128,8]{0,1:T(8,128)S(1)}, f32[128,8]{0,1:T(8,128)S(1)}, u32[]{:S(2)}, u32[]{:S(2)}) %collective-permute-start.12) | collective-permute-done | bytes 4128 | tf_op jit(solution)/shard_map/ppermute | solution.py:30
  77.3 0.0 collective-permute-start.13
  77.3 19.4 %all_gather.11 = bf16[2048,128]{0,1:T(8,128)(2,1)S(1)} all-gather(bf16[128,128]{0,1:T(8,128)(2,1)S(1)} %get-tuple-element.118), channel_id=1, replica_groups=mesh['sp'=16,'tp'=2] {'sp'}, dimensions={0}, use_global_device_ids=true | all-gather | bytes 557056 | tf_op jit(solution)/shard_map/all_gather | solution.py:36
  96.7 0.0 collective-permute-done.13
  96.8 0.2 collective-permute-start.14
  96.9 20.4 %all_gather.10 = bf16[2048,128]{0,1:T(8,128)(2,1)S(1)} all-gather(bf16[128,128]{0,1:T(8,128)(2,1)S(1)} %get-tuple-element.119), channel_id=1, replica_groups=mesh['sp'=16,'tp'=2] {'sp'}, dimensions={0}, use_global_device_ids=true | all-gather | bytes 557056 | tf_op jit(solution)/shard_map/all_gather | solution.py:35
  117.3 0.0 collective-permute-done.14
  117.5 0.0 copy-done.1
  117.7 0.0 copy-start
  117.8 0.5 copy-done
  118.4 8.9 %while.16 = (s32[]{:T(128)}, f32[128,2,4]{0,2,1:T(4,128)S(1)}, f32[128,2,4]{0,2,1:T(4,128)S(1)}, f32[128,2,4,64]{0,3,2,1:T(8,128)S(1)}, s32[]{:T(128)}, /*index=...) while((s32[]{:T(128)}, f32[128,2,4]{0,2,1:T(4,128)S(1)}, ...), condition=%wide.wide.region_3.4_spmd.clone, body=%wide.wide.region_0.3_spmd.clone.sunk | while | flops 577114240 | bytes 28210328 | solution.py:79
  118.4 0.3 broadcast_compare_fusion.3
  118.7 2.6 %fusion.57 = (f32[128,2,4]{0,2,1:T(4,128)S(1)}, f32[2,2048,128,4]{2,1,3,0:T(8,128)S(1)}) fusion(f32[2,4,2048]{2,1,0:T(4,128)S(1)} %bitcast.108, f32[128,2,4]{0,2,1:T(4,128)S(1)} %bitcast.118, pred[128,2048]{0,1:T(8,128)(4,1)S(1)} %broadcast_compare_fusion.3, bf16[2048,2,64,1]{0,2,3,1:T(8,128)(2,1)S(1)} %bitcast.114, ...), kind=kOutput, calls=%fused_computation.7.clone.clone.1 | convolution fusion | flops 278920192 | bytes 9379840 | tf_op jit(solution)/shard_map/while/body/tkgd,rkd->tkgr/dot_general | solution.py:52
  121.3 3.1 %fusion.58 = f32[128,2,4]{0,2,1:T(4,128)S(1)} fusion(f32[2,2048,128,4]{2,1,3,0:T(8,128)S(1)} %get-tuple-element.252, f32[128,2,4]{0,2,1:T(4,128)S(1)} %max.6, f32[2,4,2048]{2,1,0:T(4,128)S(1)} %bitcast.109, f32[128,2,4]{0,2,1:T(4,128)S(1)} %bitcast.119, pred[128,2048]{0,1:T(8,128)(4,1)S(1)} %broadcast_compare_fusion.3), kind=kLoop, calls=%fused_computation.6.clone.clone.1 | loop fusion | flops 14679040 | bytes 8728576 | tf_op jit(solution)/shard_map/while/body/reduce_sum | solution.py:65
  124.5 2.8 %fusion.59 = f32[128,2,4,64]{0,3,2,1:T(8,128)S(1)} fusion(bf16[2048,2,64,1]{0,2,3,1:T(8,128)(2,1)S(1)} %bitcast.113, f32[2,2048,128,4]{2,1,3,0:T(8,128)S(1)} %get-tuple-element.252, f32[128,2,4]{0,2,1:T(4,128)S(1)} %max.6, f32[2,4,2048]{2,1,0:T(4,128)S(1)} %bitcast.110, f32[128,2,4]{0,2,1:T(4,128)S(1)} %bitcast.120, ...), kind=kOutput, calls=%fused_computation.11.clone.clone.1 | convolution fusion | flops 283246592 | bytes 9777152 | tf_op jit(solution)/shard_map/while/body/tkgr,rkd->tkgd/dot_general | solution.py:66
  127.3 0.1 reshape.55
  127.5 0.1 copy.14
  127.6 7.4 %all_to_all.19 = bf16[2,64,512]{2,1,0:T(8,128)(2,1)S(1)} all-to-all(bf16[2,64,512]{2,1,0:T(8,128)(2,1)S(1)} %copy.14), channel_id=1, replica_groups=mesh['sp'=16,'tp'=2] {'tp'}, dimensions={0} | all-to-all | bytes 262144 | tf_op jit(solution)/shard_map/all_to_all | solution.py:81
  135.1 3.7 %convolution_convert_fusion = bf16[64,2048]{1,0:T(8,128)(2,1)} fusion(bf16[64,1024]{1,0:T(8,128)(2,1)S(1)} %bitcast.112, bf16[1024,2048]{1,0:T(8,128)(2,1)} %param.13), kind=kOutput, calls=%fused_computation.26 | convolution fusion | flops 268566528 | bytes 4587520 | tf_op jit(solution)/shard_map/dot_general | solution.py:82
  (46 shorter events, 0.2 us)
Async XLA Ops:
  0.0 117.5 %copy-start.1 = (f32[128,8]{0,1:T(8,128)S(1)}, f32[128,8]{0,1:T(8,128)}, u32[]{:S(2)}) copy-start(f32[128,8]{0,1:T(8,128)} %param.12) | copy-start | bytes 12292
  0.0 7.0 %collective-permute-start = (f32[128,8]{0,1:T(8,128)}, f32[128,8]{0,1:T(8,128)S(1)}, u32[]{:S(2)}, u32[]{:S(2)}) collective-permute-start(f32[128,8]{0,1:T(8,128)} %param.12), channel_id=1, source_target_pairs={{0,2},{2,4},{4,6},{6,8},{8,10},{10,12},{12,14},{14,16},{16,18},{18... | collective-permute-start | bytes 12296 | tf_op jit(solution)/shard_map/ppermute | solution.py:30
  7.0 5.7 %collective-permute-start.1 = (f32[128,8]{0,1:T(8,128)S(1)}, f32[128,8]{0,1:T(8,128)S(1)}, u32[]{:S(2)}, u32[]{:S(2)}) collective-permute-start(f32[128,8]{0,1:T(8,128)S(1)} %collective-permute-done), channel_id=1, source_target_pairs={{0,2},{2,4},{4,6},{6,8},{8,10},{10,12},{12,14},{14,16},{16,18},{18... | collective-permute-start | bytes 12296 | tf_op jit(solution)/shard_map/ppermute | solution.py:30
  12.8 5.7 %collective-permute-start.2 = (f32[128,8]{0,1:T(8,128)S(1)}, f32[128,8]{0,1:T(8,128)S(1)}, u32[]{:S(2)}, u32[]{:S(2)}) collective-permute-start(f32[128,8]{0,1:T(8,128)S(1)} %collective-permute-done.1), channel_id=1, source_target_pairs={{0,2},{2,4},{4,6},{6,8},{8,10},{10,12},{12,14},{14,16},{16,18},{18... | collective-permute-start | bytes 12296 | tf_op jit(solution)/shard_map/ppermute | solution.py:30
  18.5 5.7 %collective-permute-start.3 = (f32[128,8]{0,1:T(8,128)S(1)}, f32[128,8]{0,1:T(8,128)S(1)}, u32[]{:S(2)}, u32[]{:S(2)}) collective-permute-start(f32[128,8]{0,1:T(8,128)S(1)} %collective-permute-done.2), channel_id=1, source_target_pairs={{0,2},{2,4},{4,6},{6,8},{8,10},{10,12},{12,14},{14,16},{16,18},{18... | collective-permute-start | bytes 12296 | tf_op jit(solution)/shard_map/ppermute | solution.py:30
  24.2 5.7 %collective-permute-start.4 = (f32[128,8]{0,1:T(8,128)S(1)}, f32[128,8]{0,1:T(8,128)S(1)}, u32[]{:S(2)}, u32[]{:S(2)}) collective-permute-start(f32[128,8]{0,1:T(8,128)S(1)} %collective-permute-done.3), channel_id=1, source_target_pairs={{0,2},{2,4},{4,6},{6,8},{8,10},{10,12},{12,14},{14,16},{16,18},{18... | collective-permute-start | bytes 12296 | tf_op jit(solution)/shard_map/ppermute | solution.py:30
  30.0 5.7 %collective-permute-start.5 = (f32[128,8]{0,1:T(8,128)S(1)}, f32[128,8]{0,1:T(8,128)S(1)}, u32[]{:S(2)}, u32[]{:S(2)}) collective-permute-start(f32[128,8]{0,1:T(8,128)S(1)} %collective-permute-done.4), channel_id=1, source_target_pairs={{0,2},{2,4},{4,6},{6,8},{8,10},{10,12},{12,14},{14,16},{16,18},{18... | collective-permute-start | bytes 12296 | tf_op jit(solution)/shard_map/ppermute | solution.py:30
  35.7 5.7 %collective-permute-start.6 = (f32[128,8]{0,1:T(8,128)S(1)}, f32[128,8]{0,1:T(8,128)S(1)}, u32[]{:S(2)}, u32[]{:S(2)}) collective-permute-start(f32[128,8]{0,1:T(8,128)S(1)} %collective-permute-done.5), channel_id=1, source_target_pairs={{0,2},{2,4},{4,6},{6,8},{8,10},{10,12},{12,14},{14,16},{16,18},{18... | collective-permute-start | bytes 12296 | tf_op jit(solution)/shard_map/ppermute | solution.py:30
  41.4 5.7 %collective-permute-start.7 = (f32[128,8]{0,1:T(8,128)S(1)}, f32[128,8]{0,1:T(8,128)S(1)}, u32[]{:S(2)}, u32[]{:S(2)}) collective-permute-start(f32[128,8]{0,1:T(8,128)S(1)} %collective-permute-done.6), channel_id=1, source_target_pairs={{0,2},{2,4},{4,6},{6,8},{8,10},{10,12},{12,14},{14,16},{16,18},{18... | collective-permute-start | bytes 12296 | tf_op jit(solution)/shard_map/ppermute | solution.py:30
  47.2 5.7 %collective-permute-start.8 = (f32[128,8]{0,1:T(8,128)S(1)}, f32[128,8]{0,1:T(8,128)S(1)}, u32[]{:S(2)}, u32[]{:S(2)}) collective-permute-start(f32[128,8]{0,1:T(8,128)S(1)} %collective-permute-done.7), channel_id=1, source_target_pairs={{0,2},{2,4},{4,6},{6,8},{8,10},{10,12},{12,14},{14,16},{16,18},{18... | collective-permute-start | bytes 12296 | tf_op jit(solution)/shard_map/ppermute | solution.py:30
  52.9 5.7 %collective-permute-start.9 = (f32[128,8]{0,1:T(8,128)S(1)}, f32[128,8]{0,1:T(8,128)S(1)}, u32[]{:S(2)}, u32[]{:S(2)}) collective-permute-start(f32[128,8]{0,1:T(8,128)S(1)} %collective-permute-done.8), channel_id=1, source_target_pairs={{0,2},{2,4},{4,6},{6,8},{8,10},{10,12},{12,14},{14,16},{16,18},{18... | collective-permute-start | bytes 12296 | tf_op jit(solution)/shard_map/ppermute | solution.py:30
  58.6 7.2 %collective-permute-start.10 = (f32[128,8]{0,1:T(8,128)S(1)}, f32[128,8]{0,1:T(8,128)S(1)}, u32[]{:S(2)}, u32[]{:S(2)}) collective-permute-start(f32[128,8]{0,1:T(8,128)S(1)} %collective-permute-done.9), channel_id=1, source_target_pairs={{0,2},{2,4},{4,6},{6,8},{8,10},{10,12},{12,14},{14,16},{16,18},{18... | collective-permute-start | bytes 12296 | tf_op jit(solution)/shard_map/ppermute | solution.py:30
  65.9 5.7 %collective-permute-start.11 = (f32[128,8]{0,1:T(8,128)S(1)}, f32[128,8]{0,1:T(8,128)S(1)}, u32[]{:S(2)}, u32[]{:S(2)}) collective-permute-start(f32[128,8]{0,1:T(8,128)S(1)} %collective-permute-done.10), channel_id=1, source_target_pairs={{0,2},{2,4},{4,6},{6,8},{8,10},{10,12},{12,14},{14,16},{16,18},{18... | collective-permute-start | bytes 12296 | tf_op jit(solution)/shard_map/ppermute | solution.py:30
  71.6 5.7 %collective-permute-start.12 = (f32[128,8]{0,1:T(8,128)S(1)}, f32[128,8]{0,1:T(8,128)S(1)}, u32[]{:S(2)}, u32[]{:S(2)}) collective-permute-start(f32[128,8]{0,1:T(8,128)S(1)} %collective-permute-done.11), channel_id=1, source_target_pairs={{0,2},{2,4},{4,6},{6,8},{8,10},{10,12},{12,14},{14,16},{16,18},{18... | collective-permute-start | bytes 12296 | tf_op jit(solution)/shard_map/ppermute | solution.py:30
  77.3 19.4 %collective-permute-start.13 = (f32[128,8]{0,1:T(8,128)S(1)}, f32[128,8]{0,1:T(8,128)S(1)}, u32[]{:S(2)}, u32[]{:S(2)}) collective-permute-start(f32[128,8]{0,1:T(8,128)S(1)} %collective-permute-done.12), channel_id=1, source_target_pairs={{0,2},{2,4},{4,6},{6,8},{8,10},{10,12},{12,14},{14,16},{16,18},{18... | collective-permute-start | bytes 12296 | tf_op jit(solution)/shard_map/ppermute | solution.py:30
  96.8 20.6 %collective-permute-start.14 = (f32[128,8]{0,1:T(8,128)S(1)}, f32[128,8]{0,1:T(8,128)S(1)}, u32[]{:S(2)}, u32[]{:S(2)}) collective-permute-start(f32[128,8]{0,1:T(8,128)S(1)} %collective-permute-done.13), channel_id=1, source_target_pairs={{0,2},{2,4},{4,6},{6,8},{8,10},{10,12},{12,14},{14,16},{16,18},{18... | collective-permute-start | bytes 12296 | tf_op jit(solution)/shard_map/ppermute | solution.py:30
  117.7 0.6 copy-start
